TPU v7x, 32 devices: a whole 2x2x4 slice. The times are simulated.
32 devices in a mesh: grp: 2 (over y), sp: 4 (over z), tp: 4 (over x, core).
Axes of the slice: x: 2, y: 2, z: 4, core: 2. Of those that a mesh axis runs over, the one named last changes fastest.
Arguments:
- gate_in: bfloat16 [4096, 1536], P(('grp', 'sp'), 'tp'), parts along dimension 0, may hold values from -6 to 6
- mult_in: bfloat16 [4096, 1536], P(('grp', 'sp'), 'tp'), parts along dimension 0, may hold values from -6 to 6
- value_in: bfloat16 [4096, 1536], P(('grp', 'sp'), 'tp'), parts along dimension 0, may hold values from -6 to 6
- doc_ids: int32 [4096], P(('grp', 'sp')), parts along dimension 0, may hold values from 0 to 1, never falling along the last dimension, each value on 1 to 1536 neighbouring positions
- conv_taps: bfloat16 [3, 1536], P(None, 'tp'), may hold values from -3 to 3
- out_proj: bfloat16 [1536, 2048], P('tp'), may hold values from -0.15625 to 0.15625
- resid: bfloat16 [4096, 2048], P(('grp', 'sp', 'tp')), parts along dimension 0, may hold values from -6 to 6
- norm1_gain: float32 [2048], replicated, may hold values from 0.1 to 1.9
- norm1_bias: float32 [2048], replicated, may hold values from -1.5 to 1.5
- expert_ids: int32 [4096, 2], P(('grp', 'sp', 'tp')), parts along dimension 0, may hold values from 0 to 3, all different within a row; in each aligned block of 128 rows (0 to 127, 128 to 255, ...) at most 80 rows name the same one
- expert_wts: float32 [4096, 2], P(('grp', 'sp', 'tp')), parts along dimension 0, may hold values from 0.1 to 1
- w_gate: bfloat16 [4, 2048, 3072], P('sp', None, 'tp'), may hold values from -0.125 to 0.125
- w_up: bfloat16 [4, 2048, 3072], P('sp', None, 'tp'), may hold values from -0.125 to 0.125
- w_down: bfloat16 [4, 3072, 2048], P('sp', 'tp'), may hold values from -0.21582031 to 0.21582031
- norm2_gain: float32 [2048], replicated, may hold values from 0.1 to 1.9
- norm2_bias: float32 [2048], replicated, may hold values from -1.5 to 1.5
Outputs:
- result: bfloat16 [4096, 2048], P(('grp', 'sp', 'tp')), parts along dimension 0
There are 2 independent parts, one for each index of `grp`. A program takes and returns all parts, laid end to end along the dimension named above; an argument that names none is the same for every part. Nothing has to cross between parts.
Inputs may be any that keep to these rules, and one draw needn't show every extreme that they name: `doc_ids`: never falling along the sequence; each document has 1 to 1536 positions and one has exactly 1536. `expert_ids`: each row names 2 different experts. Among the rows of one device no expert is named more than 80 times, and in some device's rows some expert is named exactly 80 times.
All inputs are finite; a program needn't handle non-finite values.
Results may differ from a plain program's by a relative error of at most 0.0095.
Values may be sent and summed in bfloat16 or wider, within the bound.
A program may use at most 128 MiB of HBM per device.

v0:
```python
import jax
import jax.numpy as jnp
from jax import lax
from jax.sharding import PartitionSpec as P

residual_scale = 2.0**0.5
norm_eps = 1e-05


def shifted_2(x, axis, by):
    length = lax.axis_size(axis)
    pairs = [(i, i + by) for i in range(length) if 0 <= i + by < length]
    return lax.ppermute(x, axis, pairs)


def layer_norm(pre, gain, bias):
    center = pre - jnp.mean(pre, axis=-1, keepdims=True)
    spread = jnp.mean(center * center, axis=-1, keepdims=True)
    return center * lax.rsqrt(spread + norm_eps) * gain + bias


def shards(
    gate_in,
    mult_in,
    value_in,
    doc_ids,
    conv_taps,
    out_proj,
    resid,
    norm1_gain,
    norm1_bias,
    expert_ids,
    expert_wts,
    w_gate,
    w_up,
    w_down,
    norm2_gain,
    norm2_bias,
):
    tap_weights = conv_taps.astype(jnp.float32)
    kernel_width = tap_weights.shape[0]
    product = mult_in.astype(jnp.float32) * value_in.astype(jnp.float32)
    doc_numbers = doc_ids.astype(jnp.float32)
    row_count = product.shape[0]
    prev_rows, prev_docs = shifted_2(
        (product[row_count - kernel_width + 1 :], doc_numbers[row_count - kernel_width + 1 :]),
        "sp",
        1,
    )
    ext_rows = jnp.concatenate([prev_rows, product], axis=0)
    ext_docs = jnp.concatenate([prev_docs, doc_numbers], axis=0)
    filtered = jnp.zeros_like(product)
    for tap_index in range(kernel_width):
        shifted = ext_rows[tap_index : tap_index + row_count]
        same_doc = (ext_docs[tap_index : tap_index + row_count] == doc_numbers)[:, None]
        filtered = filtered + tap_weights[tap_index] * jnp.where(same_doc, shifted, 0.0)
    mixed_heads = (gate_in.astype(jnp.float32) * filtered).astype(jnp.bfloat16)
    tok_rows = lax.all_to_all(mixed_heads, "tp", split_axis=0, concat_axis=1, tiled=True)
    model_width = out_proj.shape[1]
    mixed = jnp.dot(
        tok_rows,
        lax.all_gather(out_proj, "tp", axis=0, tiled=True),
        preferred_element_type=jnp.float32,
    )
    hidden_one = layer_norm(
        residual_scale * resid.astype(jnp.float32) + mixed, norm1_gain, norm1_bias
    ).astype(jnp.bfloat16)
    tok_count = expert_ids.shape[0]
    top_count = expert_ids.shape[1]
    experts = lax.axis_size("sp")
    capacity = 5 * tok_count * top_count // (4 * experts)
    flat_ids = expert_ids.reshape(-1)
    one_hot = (flat_ids[:, None] == jnp.arange(experts, dtype=jnp.int32)[None, :]).astype(jnp.int32)
    earlier = jnp.cumsum(one_hot, axis=0) - one_hot
    slot_index = jnp.sum(earlier * one_hot, axis=1)
    dest_slot = (flat_ids * capacity + slot_index).reshape(tok_count, top_count)
    slot_ids = jnp.arange(experts * capacity, dtype=jnp.int32)
    selector = jnp.any(slot_ids[:, None, None] == dest_slot[None, :, :], axis=2).astype(
        jnp.bfloat16
    )
    packed = jnp.dot(selector, hidden_one, preferred_element_type=jnp.float32).astype(jnp.bfloat16)
    packed = packed.reshape(experts, capacity, model_width)
    whole = lax.all_gather(
        lax.all_to_all(packed, "sp", split_axis=0, concat_axis=0, tiled=True),
        "tp",
        axis=0,
        tiled=True,
    )
    shape_in = whole.shape
    rows_in = whole.reshape(-1, shape_in[-1])
    gate_act = jnp.dot(rows_in, w_gate[0], preferred_element_type=jnp.float32)
    up_act = jnp.dot(rows_in, w_up[0], preferred_element_type=jnp.float32)
    hid = (jax.nn.silu(gate_act) * up_act).astype(jnp.bfloat16)
    summed = lax.psum_scatter(
        jnp.dot(hid, w_down[0], preferred_element_type=jnp.float32)
        .astype(jnp.bfloat16)
        .reshape(shape_in),
        "tp",
        scatter_dimension=0,
        tiled=True,
    )
    expert_out = lax.all_to_all(summed, "sp", split_axis=0, concat_axis=0, tiled=True)
    expert_flat = expert_out.reshape(experts * capacity, model_width)
    picked = jnp.take(expert_flat, dest_slot, axis=0)
    moe = jnp.sum(expert_wts[:, :, None] * picked.astype(jnp.float32), axis=1)
    return layer_norm(
        residual_scale * hidden_one.astype(jnp.float32) + moe, norm2_gain, norm2_bias
    ).astype(jnp.bfloat16)


def solution(mesh):
    placed = (
        P(("grp", "sp"), "tp"),
        P(("grp", "sp"), "tp"),
        P(("grp", "sp"), "tp"),
        P(("grp", "sp")),
        P(None, "tp"),
        P("tp", None),
        P(("grp", "sp", "tp"), None),
        P(),
        P(),
        P(("grp", "sp", "tp"), None),
        P(("grp", "sp", "tp"), None),
        P("sp", None, "tp"),
        P("sp", None, "tp"),
        P("sp", "tp", None),
        P(),
        P(),
    )
    return jax.shard_map(
        shards, mesh=mesh, in_specs=placed, out_specs=P(("grp", "sp", "tp"), None), check_vma=False
    )
```

profile of v0, /device:TPU:0, one launch (start us, length us, event | category | flops | bytes accessed | tf_op | source)
XLA Modules:
  0.0 271.4 jit_solution(6513428504128763117)
XLA Ops:
  6.6 0.7 all-gather.3.cloned.1.call-update
  7.3 0.8 convert_element_type.53
  8.1 4.9 %collective-permute-start = (f32[2]{0:T(128)S(1)}, f32[2]{0:T(128)S(1)}, u32[]{:S(2)}, u32[]{:S(2)}) collective-permute-start(f32[2]{0:T(128)S(1)} %slice.34), channel_id=1, source_target_pairs={{0,4},{4,8},{8,12},{1,5},{5,9},{9,13},{2,6},{6,10},{10,14},{3,7},{... | collective-permute-start | bytes 32 | tf_op jit(solution)/shard_map/ppermute | solution.py:13
  13.1 1.2 convert_multiply_fusion
  14.3 0.9 copy-done.3
  15.2 3.5 %collective-permute-start.1 = (f32[2,384]{1,0:T(2,128)S(1)}, f32[2,384]{1,0:T(2,128)S(1)}, u32[]{:S(2)}, u32[]{:S(2)}) collective-permute-start(f32[2,384]{1,0:T(2,128)S(1)} %slice.47), channel_id=1, source_target_pairs={{0,4},{4,8},{8,12},{1,5},{5,9},{9,13},{2,6},{6,10},{10,14},{3,7},{... | collective-permute-start | bytes 9224 | tf_op jit(solution)/shard_map/ppermute | solution.py:13
  18.7 0.1 copy.56
  18.8 0.1 eq.54
  18.9 0.1 eq.50
  19.1 1.2 reduce-window.6
  20.3 0.1 slice.52
  20.4 0.1 copy.58
  20.6 0.1 copy.59
  20.7 0.1 add_bitcast_fusion
  20.8 0.1 reduce_sum.59
  21.0 0.1 pad_maximum_fusion.1
  21.1 0.1 slice_compare_fusion.1
  21.2 3.3 %fusion.11 = bf16[512,384]{1,0:T(8,128)(2,1)} fusion(f32[2,384]{1,0:T(2,128)S(1)} %collective-permute-done.1, f32[512,384]{1,0:T(8,128)} %copy-done.3, bf16[512,384]{1,0:T(8,128)(2,1)} %param.16, f32[384]{0:T(512)S(1)} %get-tuple-element.6, f32[384]{0:T(512)S(1)} %get-tuple-element.7, f32[384]{0:T(512)S(1)} %get-tuple-element.5, ...), kind=kLoop, calls=%fused_computation.25 | loop fusion | flops 2555904 | bytes 1582080 | tf_op jit(solution)/shard_map/convert_element_type | solution.py:57
  24.5 3.5 %all-to-all-start = ((bf16[4,128,384]{2,1,0:T(8,128)(2,1)}), bf16[4,128,384]{2,1,0:T(8,128)(2,1)S(1)}, u32[]{:S(2)}, u32[]{:S(2)}) async-start(bf16[4,128,384]{2,1,0:T(8,128)(2,1)} %bitcast.46), calls=%async_computation | async-start | bytes 786432 | tf_op jit(solution)/shard_map/all_to_all | solution.py:58
  28.0 0.6 compare_and_fusion
  28.6 0.6 copy-done.8
  29.1 0.7 fusion.14
  29.8 10.2 %all-to-all-done = bf16[4,128,384]{2,1,0:T(8,128)(2,1)S(1)} async-done(((bf16[4,128,384]{2,1,0:T(8,128)(2,1)}), bf16[4,128,384]{2,1,0:T(8,128)(2,1)S(1)}, u32[]{:S(2)}, u32[]{:S(2)}) %all-to-all-start) | async-done | bytes 393248 | tf_op jit(solution)/shard_map/all_to_all | solution.py:58
  40.0 0.7 copy-done.4
  40.7 1.2 copy.54
  41.9 20.3 %all-gather.3.cloned.1.call-done = bf16[1536,2048]{1,0:T(8,128)(2,1)} async-done(((bf16[384,2048]{1,0:T(8,128)(2,1)}), bf16[1536,2048]{1,0:T(8,128)(2,1)}) %all-gather.3.cloned.1.call-update) | async-done | bytes 6291472 | tf_op jit(solution)/shard_map/all_gather | solution.py:62
  62.2 4.0 %fusion.19 = (f32[128]{0:T(128)S(1)}, f32[128,2048]{1,0:T(8,128)S(1)}) fusion(bf16[128,1536]{0,1:T(8,128)(2,1)S(1)} %bitcast.44, bf16[1536,2048]{1,0:T(8,128)(2,1)} %all-gather.3.cloned.1.call-done, bf16[128,2048]{1,0:T(8,128)(2,1)} %param.22), kind=kOutput, calls=%fused_computation.55 | convolution fusion | flops 806354816 | bytes 8258048 | tf_op jit(solution)/shard_map/dot_general | solution.py:60
  66.2 0.3 multiply_reduce_fusion.2
  66.5 0.7 copy-done.1
  67.2 0.6 convolution_convert_fusion.1
  67.9 36.3 %all_to_all.29 = bf16[4,80,2048]{2,1,0:T(8,128)(2,1)} all-to-all(bf16[4,80,2048]{2,1,0:T(8,128)(2,1)S(1)} %bitcast.43), channel_id=1, replica_groups=mesh['grp'=2,'sp'=4,'tp'=4] {'sp'}, dimensions={0} | all-to-all | bytes 2621440 | tf_op jit(solution)/shard_map/all_to_all | solution.py:84
  104.2 38.6 %all-gather.5.cloned.1.call-done = bf16[16,80,2048]{2,1,0:T(8,128)(2,1)} async-done(((bf16[4,80,2048]{2,1,0:T(8,128)(2,1)}), bf16[16,80,2048]{2,1,0:T(8,128)(2,1)}) %all-gather.5.cloned.1.call-update) | async-done | bytes 5242896 | tf_op jit(solution)/shard_map/all_gather | solution.py:83
  142.8 7.2 %fusion.3 = f32[1280,768]{1,0:T(8,128)S(1)} fusion(bf16[1280,2048]{1,0:T(8,128)(2,1)} %bitcast.48, bf16[1,2048,768]{2,1,0:T(8,128)(2,1)} %param.27), kind=kOutput, calls=%fused_computation.6 | convolution fusion | flops 4026531840 | bytes 12320768 | tf_op jit(solution)/shard_map/dot_general | solution.py:91
  150.1 4.8 %fusion = bf16[1280,768]{1,0:T(8,128)(2,1)S(1)} fusion(bf16[1280,2048]{1,0:T(8,128)(2,1)S(1)} %bitcast.49, f32[1280,768]{1,0:T(8,128)S(1)} %fusion.3, bf16[1,2048,768]{2,1,0:T(8,128)(2,1)S(1)} %copy-done.18), kind=kOutput, calls=%fused_computation.3 | convolution fusion | flops 4032430080 | bytes 14286848 | tf_op jit(solution)/shard_map/dot_general | solution.py:92
  154.9 6.0 %convolution_convert_fusion = bf16[1280,2048]{1,0:T(8,128)(2,1)} fusion(bf16[1280,768]{1,0:T(8,128)(2,1)S(1)} %fusion, bf16[1,768,2048]{2,1,0:T(8,128)(2,1)S(1)} %copy-done), kind=kOutput, calls=%fused_computation.1 | convolution fusion | flops 4029153280 | bytes 10354688 | tf_op jit(solution)/shard_map/dot_general | solution.py:95
  161.0 51.5 %reduce-scatter.2.cloned.1.call-done = bf16[4,80,2048]{2,1,0:T(8,128)(2,1)} async-done(((bf16[16,80,2048]{2,1,0:T(8,128)(2,1)}), bf16[4,80,2048]{2,1,0:T(8,128)(2,1)}) %reduce-scatter.2.cloned.1.call-update) | async-done | bytes 1310736 | tf_op jit(solution)/shard_map/reduce_scatter | solution.py:94
  212.5 4.6 %all-to-all-start.2 = ((bf16[4,80,2048]{2,1,0:T(8,128)(2,1)}), bf16[4,80,2048]{2,1,0:T(8,128)(2,1)}, u32[]{:S(2)}, u32[]{:S(2)}) async-start(bf16[4,80,2048]{2,1,0:T(8,128)(2,1)} %reduce-scatter.2.cloned.1.call-done), calls=%async_computation.3 | async-start | bytes 2621440 | tf_op jit(solution)/shard_map/all_to_all | solution.py:102
  217.1 0.1 copy.62
  217.2 0.1 reshape.85
  217.4 0.1 copy.61
  217.5 0.1 copy.55
  217.7 30.7 %all-to-all-done.2 = bf16[4,80,2048]{2,1,0:T(8,128)(2,1)} async-done(((bf16[4,80,2048]{2,1,0:T(8,128)(2,1)}), bf16[4,80,2048]{2,1,0:T(8,128)(2,1)}, u32[]{:S(2)}, u32[]{:S(2)}) %all-to-all-start.2) | async-done | bytes 1310752 | tf_op jit(solution)/shard_map/all_to_all | solution.py:102
  248.4 4.8 %gather_fusion = bf16[256,2048]{1,0:T(8,128)(2,1)} fusion(bf16[320,2048]{1,0:T(8,128)(2,1)} %bitcast.11, s32[1024]{0:T(1024)S(1)} %pad_clamp_fusion), kind=kCustom, calls=%fused_computation | custom fusion | bytes 2098176 | tf_op jit(solution)/shard_map/jit(_take)/gather | solution.py:104
  253.2 2.5 reshape.84
  255.8 5.5 %multiply_reduce_fusion = f32[128,2048]{1,0:T(8,128)S(1)} fusion(bf16[128,2,2048]{2,1,0:T(2,128)(2,1)} %reshape.84, pred[128,2]{1,0:T(8,128)(4,1)S(1)} %copy.61, f32[128,2]{1,0:T(8,128)S(1)} %copy.55), kind=kLoop, calls=%fused_computation.10 | loop fusion | flops 1835008 | bytes 2098432 | tf_op jit(solution)/shard_map/reduce_sum | solution.py:105
  261.3 1.6 fusion.15
  263.0 0.5 multiply_reduce_fusion.1
  263.5 1.4 add_convert_fusion
  (56 shorter events, 0.5 us)
Async XLA Ops:
  6.5 148.4 %copy-start = (bf16[1,768,2048]{2,1,0:T(8,128)(2,1)S(1)}, bf16[1,768,2048]{2,1,0:T(8,128)(2,1)}, u32[]{:S(2)}) copy-start(bf16[1,768,2048]{2,1,0:T(8,128)(2,1)} %param.29) | copy-start | bytes 9437188
  6.5 14.6 %copy-start.12 = (s32[512]{0:T(512)S(1)}, s32[512]{0:T(512)}, u32[]{:S(2)}) copy-start(s32[512]{0:T(512)} %param.19) | copy-start | bytes 6148
  6.5 12.1 %copy-start.13 = (s32[128,2]{0,1:T(2,128)S(1)}, s32[128,2]{0,1:T(2,128)}, u32[]{:S(2)}) copy-start(s32[128,2]{0,1:T(2,128)} %param.25) | copy-start | bytes 3076
  6.5 12.5 %copy-start.14 = (bf16[3,384]{1,0:T(4,128)(2,1)S(1)}, bf16[3,384]{1,0:T(4,128)(2,1)}, u32[]{:S(2)}) copy-start(bf16[3,384]{1,0:T(4,128)(2,1)} %param.20) | copy-start | bytes 6916
  6.5 55.7 %all-gather.3.cloned.1.call-start = ((), (), s32[]{:S(2)}) async-start(), calls=%async_computation.4 | async-start | bytes 7864320 | tf_op jit(solution)/shard_map/all_gather | solution.py:62
  8.1 12.9 %collective-permute-start = (f32[2]{0:T(128)S(1)}, f32[2]{0:T(128)S(1)}, u32[]{:S(2)}, u32[]{:S(2)}) collective-permute-start(f32[2]{0:T(128)S(1)} %slice.34), channel_id=1, source_target_pairs={{0,4},{4,8},{8,12},{1,5},{5,9},{9,13},{2,6},{6,10},{10,14},{3,7},{... | collective-permute-start | bytes 32 | tf_op jit(solution)/shard_map/ppermute | solution.py:13
  14.3 0.9 copy-start.3
  15.2 6.0 %collective-permute-start.1 = (f32[2,384]{1,0:T(2,128)S(1)}, f32[2,384]{1,0:T(2,128)S(1)}, u32[]{:S(2)}, u32[]{:S(2)}) collective-permute-start(f32[2,384]{1,0:T(2,128)S(1)} %slice.47), channel_id=1, source_target_pairs={{0,4},{4,8},{8,12},{1,5},{5,9},{9,13},{2,6},{6,10},{10,14},{3,7},{... | collective-permute-start | bytes 9224 | tf_op jit(solution)/shard_map/ppermute | solution.py:13
  24.5 15.5 %all-to-all-start = ((bf16[4,128,384]{2,1,0:T(8,128)(2,1)}), bf16[4,128,384]{2,1,0:T(8,128)(2,1)S(1)}, u32[]{:S(2)}, u32[]{:S(2)}) async-start(bf16[4,128,384]{2,1,0:T(8,128)(2,1)} %bitcast.46), calls=%async_computation | async-start | bytes 786432 | tf_op jit(solution)/shard_map/all_to_all | solution.py:58
  27.9 114.9 %all-gather.5.cloned.1.call-start = ((), (), s32[]{:S(2)}) async-start(), calls=%async_computation.5 | async-start | bytes 6553600 | tf_op jit(solution)/shard_map/all_gather | solution.py:83
  28.6 0.6 copy-start.8
  40.0 0.7 copy-start.4
  62.2 5.0 %copy-start.5 = (pred[320,128]{1,0:T(8,128)(4,1)S(1)}, pred[320,128]{1,0:T(8,128)(4,1)}, u32[]{:S(2)}) copy-start(pred[320,128]{1,0:T(8,128)(4,1)} %fusion.14) | copy-start | bytes 122884
  62.2 5.0 %copy-start.6 = (f32[2048]{0:T(1024)S(1)}, f32[2048]{0:T(1024)}, u32[]{:S(2)}) copy-start(f32[2048]{0:T(1024)} %param.24) | copy-start | bytes 24580
  62.2 5.0 %copy-start.7 = (f32[2048]{0:T(1024)S(1)}, f32[2048]{0:T(1024)}, u32[]{:S(2)}) copy-start(f32[2048]{0:T(1024)} %param.23) | copy-start | bytes 24580
  66.2 1.0 copy-start.1
  104.1 108.4 %reduce-scatter.2.cloned.1.call-start = ((), (), s32[]{:S(2)}) async-start(), calls=%async_computation.6 | async-start | bytes 6553600 | tf_op jit(solution)/shard_map/reduce_scatter | solution.py:94
  142.8 7.3 %copy-start.17 = (bf16[16,80,2048]{2,1,0:T(8,128)(2,1)S(1)}, bf16[16,80,2048]{2,1,0:T(8,128)(2,1)}, u32[]{:S(2)}) copy-start(bf16[16,80,2048]{2,1,0:T(8,128)(2,1)} %all-gather.5.cloned.1.call-done) | copy-start | bytes 15728644
  142.8 7.3 %copy-start.18 = (bf16[1,2048,768]{2,1,0:T(8,128)(2,1)S(1)}, bf16[1,2048,768]{2,1,0:T(8,128)(2,1)}, u32[]{:S(2)}) copy-start(bf16[1,2048,768]{2,1,0:T(8,128)(2,1)} %param.28) | copy-start | bytes 9437188
  161.0 56.2 %copy-start.9 = (s32[128,2]{0,1:T(2,128)S(1)}, s32[128,2]{0,1:T(2,128)}, u32[]{:S(2)}) copy-start(s32[128,2]{0,1:T(2,128)} %copy-done.8) | copy-start | bytes 3076
  161.0 56.4 %copy-start.15 = (pred[128,2]{0,1:T(4,128)(4,1)S(1)}, pred[128,2]{0,1:T(4,128)(4,1)}, u32[]{:S(2)}) copy-start(pred[128,2]{0,1:T(4,128)(4,1)} %get-tuple-element.8) | copy-start | bytes 772
  161.0 56.6 %copy-start.16 = (f32[128,2]{0,1:T(2,128)S(1)}, f32[128,2]{0,1:T(2,128)}, u32[]{:S(2)}) copy-start(f32[128,2]{0,1:T(2,128)} %param.26) | copy-start | bytes 3076
  212.5 35.9 %all-to-all-start.2 = ((bf16[4,80,2048]{2,1,0:T(8,128)(2,1)}), bf16[4,80,2048]{2,1,0:T(8,128)(2,1)}, u32[]{:S(2)}, u32[]{:S(2)}) async-start(bf16[4,80,2048]{2,1,0:T(8,128)(2,1)} %reduce-scatter.2.cloned.1.call-done), calls=%async_computation.3 | async-start | bytes 2621440 | tf_op jit(solution)/shard_map/all_to_all | solution.py:102
  255.8 7.2 %copy-start.2 = (f32[128,2048]{1,0:T(8,128)S(1)}, f32[128,2048]{1,0:T(8,128)}, u32[]{:S(2)}) copy-start(f32[128,2048]{1,0:T(8,128)} %copy-done.1) | copy-start | bytes 3145732
  255.8 7.7 %copy-start.10 = (f32[2048]{0:T(1024)S(1)}, f32[2048]{0:T(1024)}, u32[]{:S(2)}) copy-start(f32[2048]{0:T(1024)} %param.31) | copy-start | bytes 24580
  255.8 7.7 %copy-start.11 = (f32[2048]{0:T(1024)S(1)}, f32[2048]{0:T(1024)}, u32[]{:S(2)}) copy-start(f32[2048]{0:T(1024)} %param.30) | copy-start | bytes 24580
Sparse Core Ops, SparseCore 0:
  8.9 53.2 all-gather.2
  104.3 38.5 all-gather.4
  161.1 51.3 reduce-scatter.1
where the time goes:
time: 272 us; the launch traced here: 271 us
  waiting for transfers between devices  152 us (56%)
  blocking collectives  36.3 us (13%)
  matrix products  22.7 us (8%)
  other arithmetic  17.3 us (6%)
  starting transfers between devices  16.6 us (6%)
  between operations  13.4 us (5%)
  local copies, waits for them, and re-layouts  13.1 us (5%)
    reduce_scatter x1, waiting for transfers between devices, shards(): lax.psum_scatter(jnp.dot(hid, w_down[0], preferred_element_type=jnp.float...  51.5 us
    all_gather x1, waiting for transfers between devices, shards(): lax.all_gather(lax.all_to_all(packed, 'sp', split_axis=0, concat_axis=0,...  38.6 us
    all_to_all x1, blocking collectives, shards(): lax.all_to_all(packed, 'sp', split_axis=0, concat_axis=0, tiled=True)  36.3 us
    all_to_all x1, waiting for transfers between devices, shards(): lax.all_to_all(summed, 'sp', split_axis=0, concat_axis=0, tiled=True)  30.7 us
    all_gather x1, waiting for transfers between devices, shards(): lax.all_gather(out_proj, 'tp', axis=0, tiled=True)  20.3 us
    all_to_all x1, waiting for transfers between devices, shards(): lax.all_to_all(mixed_heads, 'tp', split_axis=0, concat_axis=1, tiled=True)  10.2 us
    ppermute x2, starting transfers between devices, shifted_2(): return lax.ppermute(x, axis, pairs)  8.42 us
    gather x2, local copies, waits for them, and re-layouts, shards(): picked = jnp.take(expert_flat, dest_slot, axis=0)  7.38 us
  transfers between devices with their start and end apart: 7, of which 5 were waited for; matrix products, arithmetic and copies ran while one was open for 4% of the time, Pallas kernels for 0%

commit v1 on v0

v1 whole, which is shorter than its diff:
```python
import functools

import jax
import jax.numpy as jnp
from jax import lax
from jax.experimental import pallas as pl
from jax.experimental.pallas import tpu as pltpu
from jax.sharding import PartitionSpec as P

residual_scale = 2.0**0.5
norm_eps = 1e-05
MESH = pl.DeviceIdType.MESH
f32, bf16 = jnp.float32, jnp.bfloat16


def layer_norm(pre, gain, bias):
    center = pre - jnp.mean(pre, axis=-1, keepdims=True)
    spread = jnp.mean(center * center, axis=-1, keepdims=True)
    return center * lax.rsqrt(spread + norm_eps) * gain + bias


def remote(src, dst, send, recv, **where):
    return pltpu.make_async_remote_copy(
        src_ref=src, dst_ref=dst, send_sem=send, recv_sem=recv, device_id=where, device_id_type=MESH
    )


def kernel(
    experts, slots,
    gate_h, mult_h, value_h, docs_h, taps, proj_h, resid_h, gain1, bias1, ids, wts,
    w_gate_h, w_up_h, w_down_h, gain2, bias2,
    out,
    gate, mult, value, docs, proj, resid, w_gate, w_up, w_down,
    edge_m, edge_v, edge_d, ext, ext_docs, heads,
    send1, got1, send2, got2, own, hidden, slot_of, weight_of,
    packed, rows, part, hid, sum_in, sum_send, cross_in, done_out, back, moe,
    local, edge_s, edge_r, mix_s, mix_r,
    zs, zr, xs, xr, bs, br, cs, cr, r1s, r1r, r2s, r2r, r3s, r3r,
):
    s, t = lax.axis_index("sp"), lax.axis_index("tp")
    hi, lo = t // 2, t % 2
    sib, far = hi * 2 + (1 - lo), (1 - hi) * 2 + lo
    count, model = resid.shape
    length, channels = mult.shape
    taps_n = taps.shape[0]
    top = ids.shape[0]

    loads = [
        pltpu.make_async_copy(a, b, local.at[i])
        for i, (a, b) in enumerate(
            [(mult_h, mult), (value_h, value), (docs_h, docs), (gate_h, gate), (proj_h, proj),
             (resid_h, resid), (w_gate_h, w_gate), (w_up_h, w_up), (w_down_h, w_down)]
        )
    ]
    for c in loads:
        c.start()

    barrier = pltpu.get_barrier_semaphore()

    def greet(d, _):
        pl.semaphore_signal(barrier, inc=1, device_id={"sp": (s + d) % experts}, device_id_type=MESH)
        return 0

    lax.fori_loop(1, experts, greet, 0)
    pl.semaphore_signal(barrier, inc=1, device_id={"tp": sib}, device_id_type=MESH)
    pl.semaphore_signal(barrier, inc=1, device_id={"tp": far}, device_id_type=MESH)
    pl.semaphore_wait(barrier, experts + 1)

    nxt = (s + 1) % experts
    edges = [
        remote(mult_h.at[pl.ds(length - 16, 16)], edge_m, edge_s.at[0], edge_r.at[0], sp=nxt),
        remote(value_h.at[pl.ds(length - 16, 16)], edge_v, edge_s.at[1], edge_r.at[1], sp=nxt),
        remote(docs_h.at[pl.ds(length - 8, 8)], edge_d, edge_s.at[2], edge_r.at[2], sp=nxt),
    ]
    for c in edges:
        c.start()

    padded = slot_of.shape[0]
    expert_no = lax.broadcasted_iota(jnp.int32, (padded, count), 0)
    chosen = jnp.zeros((padded, count), f32)
    weight = jnp.zeros((padded, count), f32)
    for k in range(top):
        same = ids[k : k + 1, :] == expert_no
        chosen = chosen + jnp.where(same, 1.0, 0.0)
        weight = weight + jnp.where(same, wts[k : k + 1, :], 0.0)
    before = lax.broadcasted_iota(jnp.int32, (count, count), 0) < lax.broadcasted_iota(
        jnp.int32, (count, count), 1
    )
    rank = jnp.dot(chosen.astype(bf16), jnp.where(before, 1.0, 0.0).astype(bf16), preferred_element_type=f32)
    slot_of[...] = jnp.where(chosen > 0.5, rank, -1.0)
    weight_of[...] = weight

    for c in loads[:4]:
        c.wait()
    for r in range(0, length, 128):
        ext[8 + r : 8 + r + 128, :] = mult[r : r + 128, :].astype(f32) * value[r : r + 128, :].astype(f32)
    ext_docs[8:, :] = docs[...]
    for c in edges:
        c.wait_recv()
    ext[0:8, :] = (edge_m[...].astype(f32) * edge_v[...].astype(f32))[8:16, :]
    ext_docs[0:8, :] = jnp.where(s > 0, edge_d[...], -1)
    for r in range(0, length, 64):
        now = ext_docs[8 + r : 8 + r + 64, :]
        same = [ext_docs[8 + r - b : 8 + r - b + 64, :] == now for b in range(1, taps_n)]
        for c in range(0, channels, 128):
            acc = taps[taps_n - 1 :, c : c + 128] * ext[8 + r : 8 + r + 64, c : c + 128]
            for b in range(1, taps_n):
                moved = ext[8 + r - b : 8 + r - b + 64, c : c + 128]
                acc = acc + taps[taps_n - 1 - b : taps_n - b, c : c + 128] * jnp.where(same[b - 1], moved, 0.0)
            heads[r : r + 64, c : c + 128] = (gate[r : r + 64, c : c + 128].astype(f32) * acc).astype(bf16)

    loads[4].wait()
    wide = 512

    def projected(number, n):
        return jnp.dot(
            heads[pl.ds(pl.multiple_of(number * count, count), count), :], proj[:, n : n + wide],
            preferred_element_type=f32,
        )

    mix = []
    for i, h in enumerate((1 - hi, hi)):
        for n in range(0, model, wide):
            send1[i, :, n : n + wide] = projected(h * 2 + (1 - lo), n).astype(bf16)
        c = remote(send1.at[i], got1.at[i], mix_s.at[i], mix_r.at[i], tp=sib)
        c.start()
        mix.append(c)
    for n in range(0, model, wide):
        own[:, n : n + wide] = projected((1 - hi) * 2 + lo, n)
    mix[0].wait_recv()
    for n in range(0, model, wide):
        send2[:, n : n + wide] = (own[:, n : n + wide] + got1[0, :, n : n + wide].astype(f32)).astype(bf16)
    c = remote(send2, got2, mix_s.at[2], mix_r.at[2], tp=far)
    c.start()
    mix.append(c)
    for n in range(0, model, wide):
        own[:, n : n + wide] = projected(t, n)
    loads[5].wait()
    mix[1].wait_recv()
    for n in range(0, model, wide):
        q = slice(n, n + wide)
        own[:, q] = own[:, q] + got1[1, :, q].astype(f32) + residual_scale * resid[:, q].astype(f32)
    mix[2].wait_recv()
    for r in range(0, count, 32):
        q = slice(r, r + 32)
        hidden[q, :] = layer_norm(own[q, :] + got2[q, :].astype(f32), gain1[...], bias1[...]).astype(bf16)

    slot_no = lax.broadcasted_iota(jnp.int32, (slots, count), 0).astype(f32)

    def selected(e):
        return slot_no == slot_of[pl.ds(e, 1), :]

    def pack(e):
        pick = jnp.where(selected(e), 1.0, 0.0).astype(bf16)
        return jnp.dot(pick, hidden[...], preferred_element_type=f32).astype(bf16)

    def home(d):
        return (s - d + experts) % experts

    def z_out(d):
        return remote(packed.at[d], rows.at[s, lo, hi], zs.at[d], zr.at[d], sp=(s + d) % experts)

    def x_copy(d):
        block = rows.at[home(d), lo, hi]
        return remote(block, block, xs.at[d], xr.at[d], tp=far)

    def b_copy(d):
        block = rows.at[home(d), lo, hi]
        return remote(block, block, bs.at[d], br.at[d], tp=sib)

    def c_copy(d):
        block = rows.at[home(d), lo, 1 - hi]
        return remote(block, block, cs.at[d], cr.at[d], tp=sib)

    def r1_copy(d):
        return remote(part.at[home(d), 1 - lo], sum_in.at[home(d)], r1s.at[d], r1r.at[d], tp=sib)

    def r2_copy(d):
        return remote(sum_send.at[d], cross_in.at[d], r2s.at[d], r2r.at[d], tp=far)

    def r3_copy(d):
        return remote(done_out.at[d], back.at[s], r3s.at[d], r3r.at[d], sp=home(d))

    rows[s, lo, hi] = pack(s)
    x_copy(0).start()
    b_copy(0).start()

    def dispatch(d, _):
        packed[d] = pack((s + d) % experts)
        z_out(d).start()
        return 0

    lax.fori_loop(1, experts, dispatch, 0)

    for c in loads[6:]:
        c.wait()

    def experts_of(j):
        size = 4 * slots
        step = 256
        for n in range(0, w_gate.shape[1], step):
            x = rows[j].reshape(size, model)
            g = jnp.dot(x, w_gate[:, n : n + step], preferred_element_type=f32)
            u = jnp.dot(x, w_up[:, n : n + step], preferred_element_type=f32)
            hid[:, n : n + step] = (jax.nn.silu(g) * u).astype(bf16)
        for n in range(0, model, step):
            y = jnp.dot(hid[...], w_down[:, n : n + step], preferred_element_type=f32)
            part[j, :, :, :, n : n + step] = y.astype(bf16).reshape(2, 2, slots, step)

    def turn(d, _):
        @pl.when(jnp.logical_and(d > 0, d < experts))
        def _():
            z_out(d).wait_recv()
            x_copy(d).start()
            b_copy(d).start()

        @pl.when(d >= 3)
        def _():
            b = d - 3
            r2_copy(b).wait_recv()
            j = home(b)
            total = part[j, lo, hi].astype(f32) + sum_in[j, hi].astype(f32) + cross_in[b].astype(f32)
            done_out[b] = total.astype(bf16)

            @pl.when(b > 0)
            def _():
                r3_copy(b).start()

        @pl.when(jnp.logical_and(d >= 2, d < experts + 2))
        def _():
            b = d - 2
            r1_copy(b).wait_recv()
            j = home(b)
            sum_send[b] = (part[j, lo, 1 - hi].astype(f32) + sum_in[j, 1 - hi].astype(f32)).astype(bf16)
            r2_copy(b).start()

        @pl.when(jnp.logical_and(d >= 1, d < experts + 1))
        def _():
            b = d - 1
            x_copy(b).wait_recv()
            c_copy(b).start()
            b_copy(b).wait_recv()
            c_copy(b).wait_recv()
            experts_of(home(b))
            r1_copy(b).start()

        return 0

    lax.fori_loop(0, experts + 3, turn, 0)

    def weighted(e, value_of):
        pick = jnp.where(selected(e), weight_of[pl.ds(e, 1), :], 0.0)
        high = pick.astype(bf16)
        low = (pick - high.astype(f32)).astype(bf16)
        dims = (((0,), (0,)), ((), ()))
        return lax.dot_general(high, value_of, dims, preferred_element_type=f32) + lax.dot_general(
            low, value_of, dims, preferred_element_type=f32
        )

    moe[...] = residual_scale * hidden[...].astype(f32) + weighted(s, done_out[0])

    def combine(d, _):
        r3_copy(d).wait_recv()
        e = (s + d) % experts
        moe[...] += weighted(e, back[e])
        return 0

    lax.fori_loop(1, experts, combine, 0)
    for r in range(0, count, 32):
        q = slice(r, r + 32)
        out[q, :] = layer_norm(moe[q, :], gain2[...], bias2[...]).astype(bf16)

    for c in edges + mix:
        c.wait_send()

    def drain(d, _):
        for c in (x_copy, b_copy, c_copy, r1_copy, r2_copy):
            c(d).wait_send()

        @pl.when(d > 0)
        def _():
            z_out(d).wait_send()
            r3_copy(d).wait_send()

        return 0

    lax.fori_loop(0, experts, drain, 0)


def shards(
    gate_in, mult_in, value_in, doc_ids, conv_taps, out_proj, resid, norm1_gain, norm1_bias,
    expert_ids, expert_wts, w_gate, w_up, w_down, norm2_gain, norm2_bias,
):
    experts, parts = lax.axis_size("sp"), lax.axis_size("tp")
    assert parts == 4
    length, channels = mult_in.shape
    count, model = resid.shape
    top = expert_ids.shape[1]
    units = w_gate.shape[2]
    capacity = 5 * count * top // (4 * experts)
    slots = -(-capacity // 16) * 16
    padded = max(8, experts)
    docs = jnp.broadcast_to(doc_ids[:, None], (length, 128))
    vmem = pl.BlockSpec(memory_space=pltpu.VMEM)
    hbm = pl.BlockSpec(memory_space=pl.ANY)
    V = pltpu.VMEM
    sems = pltpu.SemaphoreType.DMA
    blocks = (experts, slots, model)
    return pl.pallas_call(
        functools.partial(kernel, experts, slots),
        out_shape=jax.ShapeDtypeStruct((count, model), bf16),
        in_specs=[hbm, hbm, hbm, hbm, vmem, hbm, hbm, vmem, vmem, vmem, vmem, hbm, hbm, hbm, vmem, vmem],
        out_specs=vmem,
        scratch_shapes=[
            V((length, channels), bf16), V((length, channels), bf16), V((length, channels), bf16),
            V((length, 128), jnp.int32), V((channels, model), bf16), V((count, model), bf16),
            V((model, units), bf16), V((model, units), bf16), V((units, model), bf16),
            V((16, channels), bf16), V((16, channels), bf16), V((8, 128), jnp.int32),
            V((length + 8, channels), f32), V((length + 8, 128), jnp.int32), V((length, channels), bf16),
            V((2, count, model), bf16), V((2, count, model), bf16), V((count, model), bf16),
            V((count, model), bf16), V((count, model), f32), V((count, model), bf16),
            V((padded, count), f32), V((padded, count), f32),
            V(blocks, bf16), V((experts, 2, 2, slots, model), bf16), V((experts, 2, 2, slots, model), bf16),
            V((4 * slots, units), bf16), V((experts, 2, slots, model), bf16), V(blocks, bf16),
            V(blocks, bf16), V(blocks, bf16), V(blocks, bf16), V((count, model), f32),
            sems((9,)), sems((3,)), sems((3,)), sems((3,)), sems((3,)),
        ] + [sems((experts,))] * 14,
        compiler_params=pltpu.CompilerParams(
            collective_id=0, has_side_effects=True, vmem_limit_bytes=62 * 2**20
        ),
    )(
        gate_in, mult_in, value_in, docs, conv_taps.astype(f32), out_proj, resid,
        norm1_gain[None], norm1_bias[None], expert_ids.T, expert_wts.T,
        w_gate[0], w_up[0], w_down[0], norm2_gain[None], norm2_bias[None],
    )


def solution(mesh):
    placed = (
        P(("grp", "sp"), "tp"),
        P(("grp", "sp"), "tp"),
        P(("grp", "sp"), "tp"),
        P(("grp", "sp")),
        P(None, "tp"),
        P("tp", None),
        P(("grp", "sp", "tp"), None),
        P(),
        P(),
        P(("grp", "sp", "tp"), None),
        P(("grp", "sp", "tp"), None),
        P("sp", None, "tp"),
        P("sp", None, "tp"),
        P("sp", "tp", None),
        P(),
        P(),
    )
    return jax.shard_map(
        shards, mesh=mesh, in_specs=placed, out_specs=P(("grp", "sp", "tp"), None), check_vma=False
    )
```

time: 272 us -> 122 us (0.45)
  waiting for transfers between devices: 152 us -> 0 us
  Pallas kernels: 0 us -> 116 us
  blocking collectives: 36.3 us -> 0 us
  matrix products: 22.7 us -> 0 us
  starting transfers between devices: 16.6 us -> 0 us
  other arithmetic: 17.3 us -> 1.28 us
  between operations: 13.4 us -> 0.01 us
  local copies, waits for them, and re-layouts: 13.1 us -> 3.4 us
    pallas_call x0 -> x1, Pallas kernels: none -> 116 us  [shards(): pl.pallas_call(functools.partial(kernel, experts, slots), out_shape=jax.S...]
    all_gather x2 -> x0, waiting for transfers between devices: 59 us -> none  [the longest x1 38.6 us: shards(): lax.all_gather(lax.all_to_all(packed, 'sp', split_axis=0, concat_axis=0,...]
    reduce_scatter x1 -> x0, waiting for transfers between devices: 51.5 us -> none  [shards(): lax.psum_scatter(jnp.dot(hid, w_down[0], preferred_element_type=jnp.float...]
    all_to_all x2 -> x0, waiting for transfers between devices: 40.9 us -> none  [the longest x1 30.7 us: shards(): lax.all_to_all(summed, 'sp', split_axis=0, concat_axis=0, tiled=True)]
    all_to_all x1 -> x0, blocking collectives: 36.3 us -> none  [shards(): lax.all_to_all(packed, 'sp', split_axis=0, concat_axis=0, tiled=True)]
    dot_general x5 -> x0, matrix products: 22.7 us -> none  [the longest x1 7.24 us: shards(): gate_act = jnp.dot(rows_in, w_gate[0], preferred_element_type=jnp.float32)]
    ppermute x2 -> x0, starting transfers between devices: 8.42 us -> none  [shifted_2(): return lax.ppermute(x, axis, pairs)]
    all_to_all x2 -> x0, starting transfers between devices: 8.06 us -> none  [the longest x1 4.6 us: shards(): lax.all_to_all(summed, 'sp', split_axis=0, concat_axis=0, tiled=True)]
  transfers between devices with their start and end apart: 7 -> 0, of which waited for: 5 -> 0; matrix products, arithmetic and copies ran while one was open for 4% -> 0% of each run, Pallas kernels for 0% -> 0%
where the time goes in v1:
time: 122 us; the launch traced here: 121 us
  Pallas kernels  116 us (95%)
  local copies, waits for them, and re-layouts  3.4 us (3%)
  other arithmetic  1.28 us (1%)
    pallas_call x1, Pallas kernels, shards(): pl.pallas_call(functools.partial(kernel, experts, slots), out_shape=jax.S...  116 us

profile of v1, /device:TPU:0, one launch (start us, length us, event | category | flops | bytes accessed | tf_op | source)
XLA Modules:
  0.0 120.8 jit_solution(17114344919218846871)
XLA Ops:
  0.0 1.3 %convert_element_type.3.taps = f32[3,384]{1,0:T(4,128)} convert(bf16[3,384]{1,0:T(4,128)(2,1)} %param.20) | non-fusion elementwise | flops 1152 | bytes 6912 | tf_op jit(solution)/shard_map/convert_element_type | solution.py:332
  1.3 1.5 %broadcast_in_dim.18.docs_h = s32[512,128]{1,0:T(8,128)} broadcast(s32[512]{0:T(512)} %param.19), dimensions={0} | broadcast | bytes 264192 | tf_op jit(solution)/shard_map/broadcast_in_dim | solution.py:303
  2.8 116.1 %shard_map.154 = bf16[128,2048]{1,0:T(8,128)(2,1)} custom-call(bf16[512,384]{1,0:T(8,128)(2,1)} %gate_h.1, bf16[512,384]{1,0:T(8,128)(2,1)} %mult_h.1, bf16[512,384]{1,0:T(8,128)(2,1)} %value_h.1, s32[512,128]{1,0:T(8,128)} %broadcast_in_dim.18.docs_h, f32[3,384]{1,0:T(4,128)} %convert_element_type.3.taps, bf16[384,2048]{1,0:T(8,128)(2,1)} %proj_h.1, ...), custom_call_target="tpu_custom_call" | custom-call | tf_op jit(solution)/shard_map/pallas_call | solution.py:309
  118.9 1.9 %copy.18 = bf16[128,2048]{1,0:T(8,128)(2,1)} copy(bf16[128,2048]{1,0:T(8,128)(2,1)} %shard_map.154) | data formatting | bytes 1048576

commit v2 on v1

--- a/solution.py
+++ b/solution.py
@@ -26,14 +26,14 @@
 
 
 def kernel(
-    experts, slots,
+    experts, slots, piece,
     gate_h, mult_h, value_h, docs_h, taps, proj_h, resid_h, gain1, bias1, ids, wts,
     w_gate_h, w_up_h, w_down_h, gain2, bias2,
     out,
     gate, mult, value, docs, proj, resid, w_gate, w_up, w_down,
     edge_m, edge_v, edge_d, ext, ext_docs, heads,
     send1, got1, send2, got2, own, hidden, slot_of, weight_of,
-    packed, rows, part, hid, sum_in, sum_send, cross_in, done_out, back, moe,
+    packed, rows, part, hid, sum_in, sum_send, cross_in, done_out, back, picks,
     local, edge_s, edge_r, mix_s, mix_r,
     zs, zr, xs, xr, bs, br, cs, cr, r1s, r1r, r2s, r2r, r3s, r3r,
 ):
@@ -146,6 +146,8 @@
         hidden[q, :] = layer_norm(own[q, :] + got2[q, :].astype(f32), gain1[...], bias1[...]).astype(bf16)
 
     slot_no = lax.broadcasted_iota(jnp.int32, (slots, count), 0).astype(f32)
+    mine, other = lo * 2 + hi, lo * 2 + 1 - hi
+    pieces = slots // piece
 
     def selected(e):
         return slot_no == slot_of[pl.ds(e, 1), :]
@@ -154,137 +156,160 @@
         pick = jnp.where(selected(e), 1.0, 0.0).astype(bf16)
         return jnp.dot(pick, hidden[...], preferred_element_type=f32).astype(bf16)
 
-    def home(d):
-        return (s - d + experts) % experts
-
-    def z_out(d):
-        return remote(packed.at[d], rows.at[s, lo, hi], zs.at[d], zr.at[d], sp=(s + d) % experts)
-
-    def x_copy(d):
-        block = rows.at[home(d), lo, hi]
-        return remote(block, block, xs.at[d], xr.at[d], tp=far)
-
-    def b_copy(d):
-        block = rows.at[home(d), lo, hi]
-        return remote(block, block, bs.at[d], br.at[d], tp=sib)
-
-    def c_copy(d):
-        block = rows.at[home(d), lo, 1 - hi]
-        return remote(block, block, cs.at[d], cr.at[d], tp=sib)
-
-    def r1_copy(d):
-        return remote(part.at[home(d), 1 - lo], sum_in.at[home(d)], r1s.at[d], r1r.at[d], tp=sib)
-
-    def r2_copy(d):
-        return remote(sum_send.at[d], cross_in.at[d], r2s.at[d], r2r.at[d], tp=far)
-
-    def r3_copy(d):
-        return remote(done_out.at[d], back.at[s], r3s.at[d], r3r.at[d], sp=home(d))
-
-    rows[s, lo, hi] = pack(s)
-    x_copy(0).start()
-    b_copy(0).start()
-
-    def dispatch(d, _):
-        packed[d] = pack((s + d) % experts)
-        z_out(d).start()
-        return 0
-
-    lax.fori_loop(1, experts, dispatch, 0)
-
-    for c in loads[6:]:
-        c.wait()
-
-    def experts_of(j):
-        size = 4 * slots
-        step = 256
-        for n in range(0, w_gate.shape[1], step):
-            x = rows[j].reshape(size, model)
-            g = jnp.dot(x, w_gate[:, n : n + step], preferred_element_type=f32)
-            u = jnp.dot(x, w_up[:, n : n + step], preferred_element_type=f32)
-            hid[:, n : n + step] = (jax.nn.silu(g) * u).astype(bf16)
-        for n in range(0, model, step):
-            y = jnp.dot(hid[...], w_down[:, n : n + step], preferred_element_type=f32)
-            part[j, :, :, :, n : n + step] = y.astype(bf16).reshape(2, 2, slots, step)
-
-    def turn(d, _):
-        @pl.when(jnp.logical_and(d > 0, d < experts))
-        def _():
-            z_out(d).wait_recv()
-            x_copy(d).start()
-            b_copy(d).start()
-
-        @pl.when(d >= 3)
-        def _():
-            b = d - 3
-            r2_copy(b).wait_recv()
-            j = home(b)
-            total = part[j, lo, hi].astype(f32) + sum_in[j, hi].astype(f32) + cross_in[b].astype(f32)
-            done_out[b] = total.astype(bf16)
-
-            @pl.when(b > 0)
-            def _():
-                r3_copy(b).start()
-
-        @pl.when(jnp.logical_and(d >= 2, d < experts + 2))
-        def _():
-            b = d - 2
-            r1_copy(b).wait_recv()
-            j = home(b)
-            sum_send[b] = (part[j, lo, 1 - hi].astype(f32) + sum_in[j, 1 - hi].astype(f32)).astype(bf16)
-            r2_copy(b).start()
-
-        @pl.when(jnp.logical_and(d >= 1, d < experts + 1))
-        def _():
-            b = d - 1
-            x_copy(b).wait_recv()
-            c_copy(b).start()
-            b_copy(b).wait_recv()
-            c_copy(b).wait_recv()
-            experts_of(home(b))
-            r1_copy(b).start()
-
-        return 0
-
-    lax.fori_loop(0, experts + 3, turn, 0)
-
-    def weighted(e, value_of):
+    def z_out(k, d):
+        return remote(packed.at[k, d], rows.at[k, mine, s], zs.at[k, d], zr.at[k, d], sp=(s + d) % experts)
+
+    def x_copy(k):
+        block = rows.at[k, mine]
+        return remote(block, block, xs.at[k], xr.at[k], tp=far)
+
+    def b_copy(k):
+        block = rows.at[k, mine]
+        return remote(block, block, bs.at[k], br.at[k], tp=sib)
+
+    def c_copy(k):
+        block = rows.at[k, other]
+        return remote(block, block, cs.at[k], cr.at[k], tp=sib)
+
+    def r1_copy(k):
+        return remote(part.at[k, pl.ds((1 - lo) * 2, 2)], sum_in.at[k], r1s.at[k], r1r.at[k], tp=sib)
+
+    def r2_copy(k):
+        return remote(sum_send.at[k], cross_in.at[k], r2s.at[k], r2r.at[k], tp=far)
+
+    def r3_copy(k, d):
+        to = (s - d + experts) % experts
+        return remote(done_out.at[k, to], back.at[k, s], r3s.at[k, d], r3r.at[k, d], sp=to)
+
+    def each(count_of, run):
+        def step(i, _):
+            run(i)
+            return 0
+
+        lax.fori_loop(0, count_of, step, 0)
+
+    def across(run):
+        def step(d, _):
+            run(d)
+            return 0
+
+        lax.fori_loop(1, experts, step, 0)
+
+    def pack_for(d):
+        y = pack((s + d) % experts)
+        for k in range(pieces):
+            packed[k, d] = y[k * piece : (k + 1) * piece, :]
+
+    across(pack_for)
+    each(pieces, lambda k: across(lambda d: z_out(k, d).start()))
+    y = pack(s)
+    for k in range(pieces):
+        rows[k, mine, s] = y[k * piece : (k + 1) * piece, :]
+
+    def pick_for(e):
         pick = jnp.where(selected(e), weight_of[pl.ds(e, 1), :], 0.0)
         high = pick.astype(bf16)
         low = (pick - high.astype(f32)).astype(bf16)
-        dims = (((0,), (0,)), ((), ()))
-        return lax.dot_general(high, value_of, dims, preferred_element_type=f32) + lax.dot_general(
-            low, value_of, dims, preferred_element_type=f32
+        for k in range(pieces):
+            picks[0, k, e] = high[k * piece : (k + 1) * piece, :]
+            picks[1, k, e] = low[k * piece : (k + 1) * piece, :]
+
+    each(experts, pick_for)
+    for c in loads[6:]:
+        c.wait()
+
+    whole = 4 * experts * piece
+    group = 4 if whole <= 512 else 1
+    size = group * experts * piece
+
+    def experts_of(k):
+        def step(m, _):
+            block = pl.ds(m * group, group)
+            wide_f = 256
+            for n in range(0, w_gate.shape[1], wide_f):
+                x = rows[k, block].reshape(size, model)
+                g = jnp.dot(x, w_gate[:, n : n + wide_f], preferred_element_type=f32)
+                u = jnp.dot(x, w_up[:, n : n + wide_f], preferred_element_type=f32)
+                hid[:, n : n + wide_f] = (jax.nn.silu(g) * u).astype(bf16)
+            for n in range(0, model, wide_f):
+                y = jnp.dot(hid[...], w_down[:, n : n + wide_f], preferred_element_type=f32)
+                part[k, block, :, :, n : n + wide_f] = y.astype(bf16).reshape(group, experts, piece, wide_f)
+            return 0
+
+        lax.fori_loop(0, 4 // group, step, 0)
+
+    def turn(d, _):
+        @pl.when(d < pieces)
+        def _():
+            across(lambda i: z_out(d, i).wait_recv())
+            x_copy(d).start()
+            b_copy(d).start()
+
+        @pl.when(d >= 3)
+        def _():
+            k = d - 3
+            r2_copy(k).wait_recv()
+
+            def add(j):
+                total = part[k, mine, j].astype(f32) + sum_in[k, hi, j].astype(f32) + cross_in[k, j].astype(f32)
+                done_out[k, j] = total.astype(bf16)
+
+            each(experts, add)
+            across(lambda i: r3_copy(k, i).start())
+            back[k, s] = done_out[k, s]
+
+        @pl.when(jnp.logical_and(d >= 2, d < pieces + 2))
+        def _():
+            k = d - 2
+            r1_copy(k).wait_recv()
+
+            def add(j):
+                total = part[k, other, j].astype(f32) + sum_in[k, 1 - hi, j].astype(f32)
+                sum_send[k, j] = total.astype(bf16)
+
+            each(experts, add)
+            r2_copy(k).start()
+
+        @pl.when(jnp.logical_and(d >= 1, d < pieces + 1))
+        def _():
+            k = d - 1
+            x_copy(k).wait_recv()
+            c_copy(k).start()
+            b_copy(k).wait_recv()
+            c_copy(k).wait_recv()
+            experts_of(k)
+            r1_copy(k).start()
+
+        return 0
+
+    lax.fori_loop(0, pieces + 3, turn, 0)
+
+    each(pieces, lambda k: across(lambda d: r3_copy(k, d).wait_recv()))
+    dims = (((0,), (0,)), ((), ()))
+    total_slots = pieces * experts * piece
+    high = picks[0].reshape(total_slots, count)
+    low = picks[1].reshape(total_slots, count)
+    for n in range(0, model, 512):
+        value_of = back[:, :, :, n : n + 512].reshape(total_slots, 512)
+        own[:, n : n + 512] = (
+            residual_scale * hidden[:, n : n + 512].astype(f32)
+            + lax.dot_general(high, value_of, dims, preferred_element_type=f32)
+            + lax.dot_general(low, value_of, dims, preferred_element_type=f32)
         )
-
-    moe[...] = residual_scale * hidden[...].astype(f32) + weighted(s, done_out[0])
-
-    def combine(d, _):
-        r3_copy(d).wait_recv()
-        e = (s + d) % experts
-        moe[...] += weighted(e, back[e])
-        return 0
-
-    lax.fori_loop(1, experts, combine, 0)
     for r in range(0, count, 32):
         q = slice(r, r + 32)
-        out[q, :] = layer_norm(moe[q, :], gain2[...], bias2[...]).astype(bf16)
+        out[q, :] = layer_norm(own[q, :], gain2[...], bias2[...]).astype(bf16)
 
     for c in edges + mix:
         c.wait_send()
 
-    def drain(d, _):
+    def drain(k):
         for c in (x_copy, b_copy, c_copy, r1_copy, r2_copy):
-            c(d).wait_send()
-
-        @pl.when(d > 0)
-        def _():
-            z_out(d).wait_send()
-            r3_copy(d).wait_send()
-
-        return 0
-
-    lax.fori_loop(0, experts, drain, 0)
+            c(k).wait_send()
+        across(lambda d: z_out(k, d).wait_send())
+        across(lambda d: r3_copy(k, d).wait_send())
+
+    each(pieces, drain)
 
 
 def shards(
@@ -298,16 +323,21 @@
     top = expert_ids.shape[1]
     units = w_gate.shape[2]
     capacity = 5 * count * top // (4 * experts)
-    slots = -(-capacity // 16) * 16
+    piece = 16
+    pieces = -(-capacity // piece)
+    slots = pieces * piece
     padded = max(8, experts)
     docs = jnp.broadcast_to(doc_ids[:, None], (length, 128))
     vmem = pl.BlockSpec(memory_space=pltpu.VMEM)
     hbm = pl.BlockSpec(memory_space=pl.ANY)
     V = pltpu.VMEM
     sems = pltpu.SemaphoreType.DMA
-    blocks = (experts, slots, model)
+    blocks = (pieces, experts, piece, model)
+    routed = (pieces, 4, experts, piece, model)
+    batch = 4 * experts * piece if 4 * experts * piece <= 512 else experts * piece
+    many, each_way = sems((pieces,)), sems((pieces, experts))
     return pl.pallas_call(
-        functools.partial(kernel, experts, slots),
+        functools.partial(kernel, experts, slots, piece),
         out_shape=jax.ShapeDtypeStruct((count, model), bf16),
         in_specs=[hbm, hbm, hbm, hbm, vmem, hbm, hbm, vmem, vmem, vmem, vmem, hbm, hbm, hbm, vmem, vmem],
         out_specs=vmem,
@@ -320,11 +350,13 @@
             V((2, count, model), bf16), V((2, count, model), bf16), V((count, model), bf16),
             V((count, model), bf16), V((count, model), f32), V((count, model), bf16),
             V((padded, count), f32), V((padded, count), f32),
-            V(blocks, bf16), V((experts, 2, 2, slots, model), bf16), V((experts, 2, 2, slots, model), bf16),
-            V((4 * slots, units), bf16), V((experts, 2, slots, model), bf16), V(blocks, bf16),
-            V(blocks, bf16), V(blocks, bf16), V(blocks, bf16), V((count, model), f32),
+            V(blocks, bf16), V(routed, bf16), V(routed, bf16), V((batch, units), bf16),
+            V((pieces, 2, experts, piece, model), bf16), V(blocks, bf16), V(blocks, bf16), V(blocks, bf16),
+            V(blocks, bf16), V((2, pieces, experts, piece, count), bf16),
             sems((9,)), sems((3,)), sems((3,)), sems((3,)), sems((3,)),
-        ] + [sems((experts,))] * 14,
+            each_way, each_way, many, many, many, many, many, many,
+            many, many, many, many, each_way, each_way,
+        ],
         compiler_params=pltpu.CompilerParams(
             collective_id=0, has_side_effects=True, vmem_limit_bytes=62 * 2**20
         ),

time: 122 us -> 114 us (0.934)
  Pallas kernels: 116 us -> 109 us
    pallas_call x1, Pallas kernels: 116 us -> 109 us  [shards(): pl.pallas_call(functools.partial(kernel, experts, slots, piece), out_shap...]
where the time goes in v2:
time: 114 us
  Pallas kernels  109 us (96%)
  local copies, waits for them, and re-layouts  3.4 us (3%)
  other arithmetic  1.28 us (1%)
    pallas_call x1, Pallas kernels, shards(): pl.pallas_call(functools.partial(kernel, experts, slots, piece), out_shap...  109 us

profile of v2, /device:TPU:0, one launch (start us, length us, event | category | flops | bytes accessed | tf_op | source)
XLA Modules:
  0.0 113.9 jit_solution(8860221355312109054)
XLA Ops:
  0.0 1.3 %convert_element_type.3.taps = f32[3,384]{1,0:T(4,128)} convert(bf16[3,384]{1,0:T(4,128)(2,1)} %param.20) | non-fusion elementwise | flops 1152 | bytes 6912 | tf_op jit(solution)/shard_map/convert_element_type | solution.py:364
  1.3 1.5 %broadcast_in_dim.18.docs_h = s32[512,128]{1,0:T(8,128)} broadcast(s32[512]{0:T(512)} %param.19), dimensions={0} | broadcast | bytes 264192 | tf_op jit(solution)/shard_map/broadcast_in_dim | solution.py:330
  2.8 109.3 %shard_map.154 = bf16[128,2048]{1,0:T(8,128)(2,1)} custom-call(bf16[512,384]{1,0:T(8,128)(2,1)} %gate_h.1, bf16[512,384]{1,0:T(8,128)(2,1)} %mult_h.1, bf16[512,384]{1,0:T(8,128)(2,1)} %value_h.1, s32[512,128]{1,0:T(8,128)} %broadcast_in_dim.18.docs_h, f32[3,384]{1,0:T(4,128)} %convert_element_type.3.taps, bf16[384,2048]{1,0:T(8,128)(2,1)} %proj_h.1, ...), custom_call_target="tpu_custom_call" | custom-call | tf_op jit(solution)/shard_map/pallas_call | solution.py:339
  112.1 1.9 %copy.18 = bf16[128,2048]{1,0:T(8,128)(2,1)} copy(bf16[128,2048]{1,0:T(8,128)(2,1)} %shard_map.154) | data formatting | bytes 1048576
